TPU v7x, 512 devices: a whole 4x4x16 slice. The times are simulated.
512 devices in a mesh: ep: 32 (over z, core), tp: 16 (over y, x).
Axes of the slice: x: 4, y: 4, z: 16, core: 2. Of those that a mesh axis runs over, the one named last changes fastest.
Arguments:
- tokens: bfloat16 [1024, 2048], P('ep', 'tp'), may hold values from -200 to 200
- routing: int32 [1024, 4], P('ep'), may hold values from 0 to 63, all different within a row; in each aligned block of 32 rows (0 to 31, 32 to 63, ...) at most 8 rows name the same one
- gate_weights: float32 [1024, 4], P('ep'), may hold values from 0.05 to 1
- norm_gain: float32 [2048], replicated, may hold values from 0.1 to 1.9
- w_gate: bfloat16 [64, 2048, 2048], P('ep', None, 'tp'), may hold values from -0.33007812 to 0.33007812
- w_up: bfloat16 [64, 2048, 2048], P('ep', None, 'tp'), may hold values from -0.33007812 to 0.33007812
- w_down: bfloat16 [64, 2048, 2048], P('ep', 'tp'), may hold values from -0.026489258 to 0.026489258
Outputs:
- mixed: bfloat16 [1024, 2048], P('ep', 'tp')
Inputs may be any that keep to these rules, and one draw needn't show every extreme that they name: `routing`: each token names 4 different experts. Among the 32 tokens of one index of ep no expert is named more than 8 times, a bound that some block reaches.
All inputs are finite; a program needn't handle non-finite values.
Results may differ from a plain program's by a relative error of at most 0.015.
Values may be sent and summed in bfloat16 or wider, within the bound.
A program may use at most 128 MiB of HBM per device.

v0:
```python
import jax
import jax.numpy as jnp
from jax import lax
from jax.sharding import PartitionSpec as P

D = 2048
CAP = 8
norm_eps = 1e-06
clamp_limit = 7.0
swish_alpha = 1.702


def activate(pre_gate, pre_up):
    clamped = jnp.minimum(pre_gate, clamp_limit)
    upper = jnp.clip(pre_up, -clamp_limit, clamp_limit)
    return (clamped * jax.nn.sigmoid(swish_alpha * clamped) * (upper + 1.0)).astype(jnp.bfloat16)


def per_device(tokens, routing, gate_weights, norm_gain, w_gate, w_up, w_down):
    ep_size = lax.axis_size("ep")
    exp_here = w_gate.shape[0]
    expert_count = exp_here * ep_size
    tok_rows = tokens.shape[0]
    top_count = routing.shape[1]
    col_width = tokens.shape[1]
    chosen = routing.reshape(-1)
    onehot = (chosen[:, None] == jnp.arange(expert_count, dtype=jnp.int32)[None, :]).astype(
        jnp.int32
    )
    slot_rank = jnp.sum(jnp.cumsum(onehot, axis=0) * onehot, axis=1) - 1
    slot_index = (chosen * CAP + slot_rank).reshape(tok_rows, top_count)
    slot_ids = jnp.arange(expert_count * CAP, dtype=jnp.int32)
    matches = slot_ids[:, None, None] == slot_index[None, :, :]
    placing = jnp.sum(matches.astype(jnp.float32), axis=2).astype(jnp.bfloat16)
    outgoing = jnp.dot(placing, tokens, preferred_element_type=jnp.float32).astype(jnp.bfloat16)
    outgoing = outgoing.reshape(ep_size, exp_here, CAP, col_width)
    received = lax.all_to_all(outgoing, "ep", split_axis=0, concat_axis=0, tiled=True)
    received = jnp.transpose(received, (1, 0, 2, 3)).reshape(exp_here, ep_size * CAP, col_width)
    raw = lax.all_gather(received, "tp", axis=2, tiled=True)
    wide = raw.astype(jnp.float32)
    ssq = jnp.sum(wide * wide, axis=2, keepdims=True)
    rows = (wide * lax.rsqrt(ssq / D + norm_eps) * norm_gain).astype(jnp.bfloat16)
    gate_part = jnp.einsum("erd,edf->erf", rows, w_gate, preferred_element_type=jnp.float32)
    up_part = jnp.einsum("erd,edf->erf", rows, w_up, preferred_element_type=jnp.float32)
    hidden = activate(gate_part, up_part)
    partial_value = jnp.einsum("erf,efd->erd", hidden, w_down, preferred_element_type=jnp.float32)
    summed = lax.psum_scatter(
        partial_value.astype(jnp.bfloat16), "tp", scatter_dimension=2, tiled=True
    )
    summed = jnp.transpose(summed.reshape(exp_here, ep_size, CAP, col_width), (1, 0, 2, 3))
    returned = lax.all_to_all(summed, "ep", split_axis=0, concat_axis=0, tiled=True)
    returned = returned.reshape(expert_count * CAP, col_width).astype(jnp.float32)
    combine = jnp.sum(matches.astype(jnp.float32) * gate_weights[None, :, :], axis=2)
    mixed = jnp.dot(combine.T, returned, precision=lax.Precision.HIGHEST)
    return mixed.astype(jnp.bfloat16)


def solution(mesh):
    placed = (
        P("ep", "tp"),
        P("ep", None),
        P("ep", None),
        P(),
        P("ep", None, "tp"),
        P("ep", None, "tp"),
        P("ep", "tp", None),
    )
    return jax.shard_map(
        per_device, mesh=mesh, in_specs=placed, out_specs=P("ep", "tp"), check_vma=False
    )
```

profile of v0, /device:TPU:1, one launch (start us, length us, event | category | flops | bytes accessed | tf_op | source)
XLA Modules:
  0.0 240.7 jit_solution(11151847588226632373)
XLA Ops:
  6.5 0.0 copy-start
  6.5 0.0 copy-start.2
  6.5 0.0 all-gather.2.cloned.1.call-start
  6.5 0.9 copy.42
  7.4 0.1 eq.29
  7.5 0.1 fusion.34
  7.6 0.2 reduce_window_sum.11
  7.8 0.2 select_reduce_fusion.1
  8.0 0.1 sub.7
  8.1 0.1 copy.43
  8.2 0.7 multiply_add_fusion
  8.8 0.8 convert_reduce_fusion
  9.7 0.9 convolution_convert_fusion.1
  10.6 32.4 %all_to_all.10 = bf16[32,2,8,128]{3,2,1,0:T(8,128)(2,1)S(1)} all-to-all(bf16[32,2,8,128]{3,2,1,0:T(8,128)(2,1)S(1)} %bitcast.24), channel_id=1, replica_groups=mesh['ep'=32,'tp'=16] {'ep'}, dimensions={0} | all-to-all | bytes 262144 | tf_op jit(solution)/shard_map/all_to_all | solution.py:37
  43.0 0.7 copy_bitcast_fusion
  43.6 0.0 all-gather.2.cloned.1.call-update
  43.6 0.0 reduce-scatter.4.cloned.1.call-start
  43.7 53.2 %all-gather.2.cloned.1.call-done = bf16[2,256,2048]{2,1,0:T(8,128)(2,1)} async-done(((bf16[2,256,128]{2,1,0:T(8,128)(2,1)}), bf16[2,256,2048]{2,1,0:T(8,128)(2,1)}) %all-gather.2.cloned.1.call-update) | async-done | bytes 2097168 | tf_op jit(solution)/shard_map/all_gather | solution.py:39
  96.9 2.2 fusion
  99.1 0.0 copy-done.2
  99.1 0.0 copy-done.1
  99.1 2.0 fusion.7
  101.2 0.0 copy-done
  101.2 4.0 %convolution_convert_fusion = bf16[2,256,2048]{2,1,0:T(8,128)(2,1)} fusion(bf16[2,128,2048]{2,1,0:T(8,128)(2,1)S(1)} %copy-done, bf16[2,2048,128]{2,1,0:T(8,128)(2,1)} %param.12, bf16[2,256,2048]{2,1,0:T(8,128)(2,1)S(1)} %copy-done.1, f32[2048]{0:T(1024)S(1)} %copy-done.2, f32[2,256]{1,0:T(2,128)S(1)} %add_rsqrt_fusion, f32[2,256,128]{2,1,0:T(8,128)S(1)} %fusion.7), kind=kOutput, calls=%fused_computation.5 | convolution fusion | flops 542703616 | bytes 6563840 | tf_op jit(solution)/shard_map/erf,efd->erd/dot_general | solution.py:46
  105.2 4.8 %copy.46 = bf16[2,256,2048]{1,0,2:T(2,128)(2,1)S(1)} copy(bf16[2,256,2048]{2,1,0:T(8,128)(2,1)} %convolution_convert_fusion) | data formatting | bytes 4194304
  110.0 1.8 copy.48
  111.8 0.0 reduce-scatter.4.cloned.1.call-update
  111.8 89.9 %reduce-scatter.4.cloned.1.call-done = bf16[128,512]{1,0:T(8,128)(2,1)} async-done(((bf16[2048,512]{1,0:T(8,128)(2,1)}), bf16[128,512]{1,0:T(8,128)(2,1)}) %reduce-scatter.4.cloned.1.call-update) | async-done | bytes 131088
  201.7 0.9 reshape.38
  202.6 0.1 copy.47
  202.8 30.3 %all_to_all.11 = bf16[32,2,8,128]{3,2,1,0:T(8,128)(2,1)S(1)} all-to-all(bf16[32,2,8,128]{3,2,1,0:T(8,128)(2,1)S(1)} %copy.45), channel_id=1, replica_groups=mesh['ep'=32,'tp'=16] {'ep'}, dimensions={0} | all-to-all | bytes 262144 | tf_op jit(solution)/shard_map/all_to_all | solution.py:51
  233.1 0.8 convolution_convert_fusion.2
  (4 shorter events, 0.0 us)
Async XLA Ops:
  6.5 94.6 %copy-start = (bf16[2,128,2048]{2,1,0:T(8,128)(2,1)S(1)}, bf16[2,128,2048]{2,1,0:T(8,128)(2,1)}, u32[]{:S(2)}) copy-start(bf16[2,128,2048]{2,1,0:T(8,128)(2,1)} %param.13) | copy-start | bytes 3145732
  6.5 92.6 %copy-start.2 = (f32[2048]{0:T(1024)S(1)}, f32[2048]{0:T(1024)}, u32[]{:S(2)}) copy-start(f32[2048]{0:T(1024)} %param.10) | copy-start | bytes 24580
  6.5 90.3 %all-gather.2.cloned.1.call-start = ((), (), s32[]{:S(2)}) async-start(), calls=%async_computation.3 | async-start | bytes 2228224 | tf_op jit(solution)/shard_map/all_gather | solution.py:39
  43.6 158.0 %reduce-scatter.4.cloned.1.call-start = ((), (), s32[]{:S(2)}) async-start(), calls=%async_computation.4 | async-start | bytes 2228224
  96.9 2.2 copy-start.1
Sparse Core Ops, SparseCore 0:
  43.8 53.0 all-gather.1
  112.0 89.6 reduce-scatter.3
where the time goes:
time: 241 us
  waiting for transfers between devices  143 us (59%)
  blocking collectives  62.7 us (26%)
  between operations  13.5 us (6%)
  local copies, waits for them, and re-layouts  9.54 us (4%)
  matrix products  7.72 us (3%)
  other arithmetic  4.16 us (2%)
    unnamed x3, waiting for transfers between devices  89.9 us
    all_gather x1, waiting for transfers between devices, per_device(): raw = lax.all_gather(received, 'tp', axis=2, tiled=True)  53.2 us
    all_to_all x1, blocking collectives, per_device(): lax.all_to_all(outgoing, 'ep', split_axis=0, concat_axis=0, tiled=True)  32.4 us
    all_to_all x1, blocking collectives, per_device(): lax.all_to_all(summed, 'ep', split_axis=0, concat_axis=0, tiled=True)  30.3 us
    unnamed x11, local copies, waits for them, and re-layouts  8.58 us
  transfers between devices with their start and end apart: 2, of which 2 were waited for; matrix products, arithmetic and copies ran while one was open for 0% of the time, Pallas kernels for 0%

commit v1 on v0

--- a/solution.py
+++ b/solution.py
@@ -36,7 +36,15 @@
     outgoing = outgoing.reshape(ep_size, exp_here, CAP, col_width)
     received = lax.all_to_all(outgoing, "ep", split_axis=0, concat_axis=0, tiled=True)
     received = jnp.transpose(received, (1, 0, 2, 3)).reshape(exp_here, ep_size * CAP, col_width)
-    raw = lax.all_gather(received, "tp", axis=2, tiled=True)
+    raw = jnp.concatenate(
+        jax.lax.all_to_all(
+            jnp.stack([received] * jax.lax.psum(1, axis_name="tp"), 0),
+            axis_name="tp",
+            split_axis=0,
+            concat_axis=0,
+        ),
+        2,
+    )
     wide = raw.astype(jnp.float32)
     ssq = jnp.sum(wide * wide, axis=2, keepdims=True)
     rows = (wide * lax.rsqrt(ssq / D + norm_eps) * norm_gain).astype(jnp.bfloat16)

time: 241 us -> 214 us (0.89)
  waiting for transfers between devices: 143 us -> 80.1 us
  blocking collectives: 62.7 us -> 96.2 us
  local copies, waits for them, and re-layouts: 9.54 us -> 14.4 us
    all_gather x1 -> x0, waiting for transfers between devices: 53.2 us -> none  [per_device(): raw = lax.all_gather(received, 'tp', axis=2, tiled=True)]
    all_to_all x0 -> x1, blocking collectives: none -> 33.5 us  [per_device(): jax.lax.all_to_all(jnp.stack([received] * jax.lax.psum(1, axis_name='tp')...]
    unnamed x3 -> x2, waiting for transfers between devices: 89.9 us -> 80.1 us
    all_to_all x0 -> x2, local copies, waits for them, and re-layouts: none -> 2.86 us  [the longest x1 2.85 us: per_device(): jax.lax.all_to_all(jnp.stack([received] * jax.lax.psum(1, axis_name='tp')...]
    unnamed x11 -> x13, local copies, waits for them, and re-layouts: 8.58 us -> 10.8 us
  transfers between devices with their start and end apart: 2 -> 1, of which waited for: 2 -> 1; matrix products, arithmetic and copies ran while one was open for 0% -> 0% of each run, Pallas kernels for 0% -> 0%
where the time goes in v1:
time: 214 us; the launch traced here: 213 us
  blocking collectives  96.2 us (45%)
  waiting for transfers between devices  80.1 us (37%)
  local copies, waits for them, and re-layouts  14.4 us (7%)
  between operations  13.5 us (6%)
  matrix products  5.85 us (3%)
  other arithmetic  2.92 us (1%)
    unnamed x2, waiting for transfers between devices  80.1 us
    all_to_all x1, blocking collectives, per_device(): jax.lax.all_to_all(jnp.stack([received] * jax.lax.psum(1, axis_name='tp')...  33.5 us
    all_to_all x1, blocking collectives, per_device(): lax.all_to_all(outgoing, 'ep', split_axis=0, concat_axis=0, tiled=True)  32.4 us
    all_to_all x1, blocking collectives, per_device(): lax.all_to_all(summed, 'ep', split_axis=0, concat_axis=0, tiled=True)  30.3 us
    unnamed x13, local copies, waits for them, and re-layouts  10.8 us
  transfers between devices with their start and end apart: 1, of which 1 were waited for; matrix products, arithmetic and copies ran while one was open for 0% of the time, Pallas kernels for 0%

profile of v1, /device:TPU:1, one launch (start us, length us, event | category | flops | bytes accessed | tf_op | source)
XLA Modules:
  0.0 213.0 jit_solution(10194552313985877021)
XLA Ops:
  6.5 0.0 copy-start
  6.5 0.0 reduce-scatter.4.cloned.1.call-start
  6.5 0.8 copy.50
  7.4 0.1 eq.29
  7.5 0.1 fusion.15
  7.6 0.2 reduce_window_sum.11
  7.8 0.2 select_reduce_fusion.1
  8.0 0.1 sub.7
  8.1 0.1 copy.51
  8.1 0.7 multiply_add_fusion
  8.8 0.8 convert_reduce_fusion
  9.6 0.9 convolution_convert_fusion.1
  10.6 32.4 %all_to_all.15 = bf16[32,2,8,128]{3,2,1,0:T(8,128)(2,1)S(1)} all-to-all(bf16[32,2,8,128]{3,2,1,0:T(8,128)(2,1)S(1)} %bitcast.35), channel_id=1, replica_groups=mesh['ep'=32,'tp'=16] {'ep'}, dimensions={0} | all-to-all | bytes 262144 | tf_op jit(solution)/shard_map/all_to_all | solution.py:37
  43.0 0.5 stack.3
  43.4 33.5 %all_to_all.16 = bf16[16,2,256,128]{3,2,1,0:T(8,128)(2,1)} all-to-all(bf16[16,2,256,128]{3,2,1,0:T(8,128)(2,1)S(1)} %stack.3), channel_id=1, replica_groups=mesh['ep'=32,'tp'=16] {'tp'}, dimensions={0} | all-to-all | bytes 4194304 | tf_op jit(solution)/shard_map/all_to_all | solution.py:40
  77.0 2.9 %copy.53 = bf16[16,2,256,128]{2,3,0,1:T(8,128)(2,1)S(1)} copy(bf16[16,2,256,128]{3,2,1,0:T(8,128)(2,1)} %all_to_all.16) | data formatting | bytes 4194304 | tf_op jit(solution)/shard_map/all_to_all | solution.py:40
  79.8 0.0 copy-start.3
  79.8 0.5 multiply_reduce_fusion
  80.3 0.2 copy-done.3
  80.5 0.5 fusion.1
  81.0 0.0 copy-start.1
  81.0 1.3 copy-done.1
  82.4 0.9 convolution_minimum_fusion
  83.3 3.2 %convolution_convert_fusion = bf16[2,256,2048]{2,1,0:T(8,128)(2,1)S(1)} fusion(bf16[2,128,2048]{2,1,0:T(8,128)(2,1)S(1)} %copy-done, bf16[2,256,2048]{1,2,0:T(8,128)(2,1)} %copy-done.1, bf16[2,2048,128]{2,1,0:T(8,128)(2,1)} %param.12, f32[2,256,128]{2,1,0:T(8,128)S(1)} %convolution_minimum_fusion), kind=kOutput, calls=%fused_computation.4 | convolution fusion | flops 538509312 | bytes 6553600 | tf_op jit(solution)/shard_map/erf,efd->erd/dot_general | solution.py:54
  86.6 3.9 %copy.59 = bf16[2,256,2048]{1,0,2:T(2,128)(2,1)} copy(bf16[2,256,2048]{2,1,0:T(8,128)(2,1)S(1)} %convolution_convert_fusion) | data formatting | bytes 4194304
  90.5 3.4 %copy.61 = bf16[256,8,2,256]{3,1,2,0:T(8,128)(2,1)} copy(bf16[256,8,2,256]{3,2,1,0:T(2,128)(2,1)} %bitcast.32) | data formatting | bytes 4194304
  93.8 0.0 reduce-scatter.4.cloned.1.call-update
  93.9 80.1 %reduce-scatter.4.cloned.1.call-done = bf16[128,512]{1,0:T(8,128)(2,1)} async-done(((bf16[2048,512]{1,0:T(8,128)(2,1)}), bf16[128,512]{1,0:T(8,128)(2,1)}) %reduce-scatter.4.cloned.1.call-update) | async-done | bytes 131088
  174.0 0.9 reshape.41
  174.9 0.1 copy.60
  175.1 30.3 %all_to_all.17 = bf16[32,2,8,128]{3,2,1,0:T(8,128)(2,1)S(1)} all-to-all(bf16[32,2,8,128]{3,2,1,0:T(8,128)(2,1)S(1)} %copy.56), channel_id=1, replica_groups=mesh['ep'=32,'tp'=16] {'ep'}, dimensions={0} | all-to-all | bytes 262144 | tf_op jit(solution)/shard_map/all_to_all | solution.py:59
  205.4 0.8 convolution_convert_fusion.2
  (7 shorter events, 0.1 us)
Async XLA Ops:
  6.5 76.8 %copy-start = (bf16[2,128,2048]{2,1,0:T(8,128)(2,1)S(1)}, bf16[2,128,2048]{2,1,0:T(8,128)(2,1)}, u32[]{:S(2)}) copy-start(bf16[2,128,2048]{2,1,0:T(8,128)(2,1)} %param.13) | copy-start | bytes 3145732
  6.5 167.4 %reduce-scatter.4.cloned.1.call-start = ((), (), s32[]{:S(2)}) async-start(), calls=%async_computation.4 | async-start | bytes 2228224
  79.8 0.7 copy-start.3
  80.5 1.9 copy-start.2
  81.0 1.4 copy-start.1
Sparse Core Ops, SparseCore 0:
  94.0 79.9 reduce-scatter.3
